TPU v7x, 32 devices: a whole 2x2x4 slice. The times are simulated.
32 devices in a mesh: ep: 4 (over y, x), tp: 8 (over z, core).
Axes of the slice: x: 2, y: 2, z: 4, core: 2. Of those that a mesh axis runs over, the one named last changes fastest.
Arguments:
- tokens: bfloat16 [1024, 2048], P('ep', 'tp'), may hold values from -600 to 600
- pre_gain: float32 [2048], P('tp'), may hold values from 0.1 to 1.9
- expert_gate: bfloat16 [4, 2048, 8192], P('ep', None, 'tp'), may hold values from -0.125 to 0.125
- expert_up: bfloat16 [4, 2048, 8192], P('ep', None, 'tp'), may hold values from -0.125 to 0.125
- expert_down: bfloat16 [4, 8192, 2048], P('ep', 'tp'), may hold values from -8 to 8
- routes: int32 [1024, 2], P('ep'), may hold values from 0 to 3, all different within a row; in each aligned block of 256 rows (0 to 255, 256 to 511, ...) at most 192 rows name the same one
- route_weights: float32 [1024, 2], P('ep'), may hold values from 0.1 to 1
- post_gain: float32 [2048], P('tp'), may hold values from 0.1 to 1.9
Outputs:
- layer_out: bfloat16 [1024, 2048], P('ep', 'tp')
Inputs may be any that keep to these rules, and one draw needn't show every extreme that they name: `routes`: each token names 2 different experts. Among the 256 tokens of one index of ep no expert is named more than 192 times, a bound that some expert reaches in some of these blocks.
All inputs are finite; a program needn't handle non-finite values.
Results may differ from a plain program's by a relative error of at most 0.024.
Values may be sent and summed in bfloat16 or wider, within the bound.
A program may use at most 64 MiB of HBM per device.

v0:
```python
import functools

import jax
import jax.numpy as jnp
from jax import lax
from jax.experimental import pallas as pl
from jax.experimental.pallas import tpu as pltpu
from jax.sharding import PartitionSpec as P

EPSILON = 1e-06


def local(tokens, pre_gain, expert_gate, expert_up, expert_down, routes, route_weights, post_gain):
    local_experts = expert_gate.shape[0]
    groups = lax.axis_size("ep")
    experts_all = local_experts * groups
    tok_rows, part_width = tokens.shape
    full_width = part_width * lax.axis_size("tp")
    capacity = 3 * tok_rows // experts_all
    values = tokens.astype(jnp.float32)
    input_sq = lax.psum(jnp.sum(values * values, axis=-1), "tp")
    normed = (
        values * lax.rsqrt(input_sq / full_width + EPSILON)[:, None] * pre_gain[None, :]
    ).astype(jnp.bfloat16)
    onehot = (routes[:, :, None] == jnp.arange(experts_all, dtype=jnp.int32)).astype(jnp.int32)
    onehot = onehot.reshape(tok_rows * 2, experts_all)
    earlier = jnp.cumsum(onehot, axis=0) - onehot
    slots = jnp.sum(earlier * onehot, axis=-1).reshape(tok_rows, 2)
    positions = routes * capacity + slots
    places = jnp.arange(experts_all * capacity, dtype=jnp.int32)
    first_pick = (places[:, None] == positions[None, :, 0]).astype(jnp.bfloat16)
    second_pick = (places[:, None] == positions[None, :, 1]).astype(jnp.bfloat16)
    dispatch = first_pick + second_pick
    outgoing = jnp.dot(dispatch, normed, preferred_element_type=jnp.float32).astype(jnp.bfloat16)
    arrived = lax.all_to_all(outgoing, "ep", split_axis=0, concat_axis=0, tiled=True)
    fragment = lax.all_gather(arrived, "tp", axis=1, tiled=True)
    count = fragment.shape[1]
    grouped = fragment.reshape(groups, local_experts, capacity, count)
    gate_pre = jnp.einsum(
        "secw,ewf->secf", grouped, expert_gate, preferred_element_type=jnp.float32
    )
    up_pre = jnp.einsum("secw,ewf->secf", grouped, expert_up, preferred_element_type=jnp.float32)
    hidden = (jax.nn.silu(gate_pre) * up_pre).astype(jnp.bfloat16)
    product = jnp.einsum("secf,efd->dsec", hidden, expert_down, preferred_element_type=jnp.float32)
    summed = lax.psum_scatter(
        product.reshape(lax.axis_size("tp") * part_width, groups * local_experts * capacity).astype(
            jnp.bfloat16
        ),
        "tp",
        scatter_dimension=0,
        tiled=True,
    )
    returned = lax.all_to_all(summed, "ep", split_axis=1, concat_axis=1, tiled=True)
    contract = (((0,), (1,)), ((), ()))
    first_out = lax.dot_general(first_pick, returned, contract, preferred_element_type=jnp.float32)
    second_out = lax.dot_general(
        second_pick, returned, contract, preferred_element_type=jnp.float32
    )
    combined = route_weights[:, 0:1] * first_out + route_weights[:, 1:2] * second_out
    output_sq = lax.psum(jnp.sum(combined * combined, axis=-1), "tp")
    scaled = combined * lax.rsqrt(output_sq / full_width + EPSILON)[:, None] * post_gain[None, :]
    return scaled.astype(jnp.bfloat16)


CORES = 2
F32 = jnp.float32
BF16 = jnp.bfloat16
EXACT = lax.Precision.HIGHEST
MESH = pl.DeviceIdType.MESH


def flip(index, bits):
    place = 1
    while place <= bits:
        if bits & place:
            index = index + place - 2 * place * lax.rem(lax.div(index, place), 2)
        place *= 2
    return index


def flip_traced(index, bits, size):
    total, place = 0, 1
    while place < size:
        total = total + place * lax.rem(lax.div(index, place) + lax.div(bits, place), 2)
        place *= 2
    return total


def fused(
    groups, parts, tok, gain, route, weight, gate_hbm, up_hbm, down_hbm, post, out,
    zbuf, gains, disp, mix, hi, lo, xsend, x, squares, gate, up, down, acc_gate, acc_up,
    hidden, half, own, half_in, back, ret, zsend, zin, stats,
    wsem, zs, zr, gs, gr, xs, xr, fs, fr, ds, dr, qs, qr, cs, cr, ps, pr,
):
    t, e = lax.axis_index("tp"), lax.axis_index("ep")
    z, c = lax.div(t, CORES), lax.rem(t, CORES)
    levels = parts // CORES
    rows, width = tok.shape
    cap = disp.shape[1]
    full = parts * width

    barrier = pltpu.get_barrier_semaphore()
    for i in range(1, parts):
        pl.semaphore_signal(barrier, inc=1, device_id={"tp": flip(t, i)}, device_id_type=MESH)
    for d in range(1, groups):
        pl.semaphore_signal(barrier, inc=1, device_id={"ep": flip(e, d)}, device_id_type=MESH)

    loads = [
        pltpu.make_async_copy(gate_hbm.at[0], gate, wsem.at[0]),
        pltpu.make_async_copy(up_hbm.at[0], up, wsem.at[1]),
        pltpu.make_async_copy(down_hbm.at[0], down, wsem.at[2]),
    ]
    for load in loads:
        load.start()

    def remote(src, dst, send, recv, **device):
        return pltpu.make_async_remote_copy(
            src_ref=src, dst_ref=dst, send_sem=send, recv_sem=recv,
            device_id=device, device_id_type=MESH,
        )

    def token_copy(level, up):
        step = 1 if up else -1
        source = zbuf.at[level]
        return remote(source, source, zs.at[level, int(up)], zr.at[level], tp=t + step * CORES)

    def relay(k):
        @pl.when(z >= k)
        def _():
            if k:
                token_copy(z - k, True).wait_recv()

            @pl.when(z < levels - 1)
            def _():
                token_copy(z - k, True).start()

        @pl.when(z + k < levels)
        def _():
            if k:
                token_copy(z + k, False).wait_recv()

            @pl.when(z > 0)
            def _():
                token_copy(z + k, False).start()

    def gain_copy(i, part):
        return remote(gain, gains.at[part], gs.at[i], gr.at[part], tp=flip(t, i))

    def row_copy(j, d, source):
        level = flip(z, j)
        return remote(
            xsend.at[j, d], x.at[level * CORES + c, source],
            xs.at[j, d], xr.at[level, source], ep=flip(e, d),
        )

    def core_copy(level, source, core):
        slot = x.at[level * CORES + core, source]
        return remote(slot, slot, fs.at[level, source], fr.at[level, source], tp=z * CORES + 1 - c)

    def half_copy(source):
        return remote(
            half.at[source], half_in.at[source], ds.at[source], dr.at[source],
            tp=z * CORES + 1 - c,
        )

    def back_copy(level, source, expert):
        return remote(
            back.at[source, level], ret.at[level, expert],
            qs.at[source, level], qr.at[level, expert], ep=source,
        )

    def sum_copy(j, level):
        return remote(zsend.at[j], zin.at[level], cs.at[j], cr.at[level], tp=flip(z, j) * CORES + c)

    def stat_copy(i, part):
        return remote(stats.at[t], stats.at[part], ps.at[i], pr.at[part], tp=flip(t, i))

    zbuf[z] = tok[...]
    gains[t] = gain[...]
    r = route[...]
    first, second = r[0:1], r[1:2]
    w = weight[...]
    names = lax.broadcasted_iota(jnp.int32, (8, rows), 0)
    member = jnp.where((names == first) | (names == second), 1.0, 0.0)
    before = jnp.where(
        lax.broadcasted_iota(jnp.int32, (rows, rows), 0)
        < lax.broadcasted_iota(jnp.int32, (rows, rows), 1),
        1.0, 0.0,
    )
    slots = jnp.dot(member.astype(BF16), before.astype(BF16), preferred_element_type=F32)
    slots = jnp.where(member > 0.5, slots, -1.0).astype(jnp.int32)
    lines = lax.broadcasted_iota(jnp.int32, (cap, rows), 0)
    for k in range(groups):
        disp[k] = jnp.where(lines == slots[k : k + 1], 1.0, 0.0).astype(BF16)

    pl.semaphore_wait(barrier, parts + groups - 2)
    relay(0)

    def send(j):
        level = flip(z, j)
        if j > 0:
            relay(j)
        block = zbuf[level]
        for d in range(groups - 1, -1, -1):
            picked = jnp.dot(disp[flip(e, d)], block, preferred_element_type=F32).astype(BF16)
            if d:
                xsend[j, d] = picked
                row_copy(j, d, e).start()
            else:
                x[level * CORES + c, e] = picked
                core_copy(level, e, c).start()

    def pass_on(j):
        level = flip(z, j)
        for d in range(groups - 1, 0, -1):
            source = flip(e, d)
            row_copy(j, d, source).wait_recv()
            core_copy(level, source, c).start()

    def project(j, source):
        level = flip(z, j)
        core_copy(level, source, 1 - c).wait_recv()
        total, gate_part, up_part = None, None, None
        for core in range(CORES):
            part = level * CORES + core
            values = x[part, source].astype(F32)
            square = values * values
            for lane in range(0, width, 128):
                piece = square[:, lane : lane + 128]
                total = piece if total is None else total + piece
            scaled = (values * gains[part]).astype(BF16)
            depth = pl.ds(pl.multiple_of(part * width, 128), width)
            gate_new = jnp.dot(scaled, gate[depth, :], preferred_element_type=F32)
            up_new = jnp.dot(scaled, up[depth, :], preferred_element_type=F32)
            gate_part = gate_new if gate_part is None else gate_part + gate_new
            up_part = up_new if up_part is None else up_part + up_new
        if j > 0:
            total = total + squares[source]
            gate_part = gate_part + acc_gate[source]
            up_part = up_part + acc_up[source]
        return total, gate_part, up_part

    def collect(j):
        def body(i, carry):
            source = flip_traced(e, groups - 1 - i, groups)
            squares[source], acc_gate[source], acc_up[source] = project(j, source)
            return carry

        pass_on(j)
        lax.fori_loop(0, groups, body, 0)

    send(0)
    for i in range(1, parts):
        gain_copy(i, t).start()
    for k in range(groups):
        chosen = jnp.where(first == k, w[0:1], w[1:2])
        mix[k * cap : (k + 1) * cap, :] = jnp.where(lines == slots[k : k + 1], chosen, 0.0)
    turned = mix[...].T
    high = turned.astype(BF16)
    hi[...] = high
    lo[...] = (turned - high.astype(F32)).astype(BF16)
    for j in range(1, levels):
        send(j)
        if j == 1:
            for i in range(1, parts):
                gain_copy(i, flip(t, i)).wait_recv()
            loads[0].wait()
            loads[1].wait()
        collect(j - 1)

    def reduce(source):
        half_copy(source).wait_recv()
        for j in range(levels - 1, -1, -1):
            level = flip(z, j)
            summed = (own[source, level] + half_in[source, level].astype(F32)).astype(BF16)
            yield j, level, summed

    def expert(i, carry):
        source = flip_traced(e, groups - 1 - i, groups)
        total, gate_part, up_part = project(levels - 1, source)
        scale = lax.rsqrt(jnp.sum(total, axis=1, keepdims=True) / full + EPSILON)
        gate_part = gate_part * scale
        hidden[...] = (
            gate_part / (1.0 + jnp.exp(-gate_part)) * (up_part * scale)
        ).astype(BF16)

        def down_block(level, core):
            columns = pl.ds(pl.multiple_of((level * CORES + core) * width, 128), width)
            return jnp.dot(hidden[...], down[:, columns], preferred_element_type=F32)

        for level in range(levels):
            half[source, level] = down_block(level, 1 - c).astype(BF16)
        half_copy(source).start()
        for level in range(levels):
            own[source, level] = down_block(level, c)

        @pl.when(i > 0)
        def _():
            earlier = flip_traced(e, groups - i, groups)
            for _, level, summed in reduce(earlier):
                back[earlier, level] = summed
                back_copy(level, earlier, e).start()

        return carry

    pass_on(levels - 1)
    loads[2].wait()
    lax.fori_loop(0, groups, expert, 0)
    for _, level, summed in reduce(e):
        ret[level, e] = summed

    combined = None
    for j in range(levels - 1, -1, -1):
        level = flip(z, j)
        for d in range(groups - 1, 0, -1):
            source = flip(e, d)
            back_copy(level, source, source).wait_recv()
        results = ret[level].reshape(groups * cap, width)
        combined = jnp.dot(hi[...], results, preferred_element_type=F32) + jnp.dot(
            lo[...], results, preferred_element_type=F32
        )
        if j:
            zsend[j] = combined.astype(BF16)
            sum_copy(j, z).start()
    for j in range(levels - 1, 0, -1):
        level = flip(z, j)
        sum_copy(j, level).wait_recv()
        combined = combined + zin[level].astype(F32)
    stats[t] = lax.dot_general(
        jnp.ones((8, width), F32), combined * combined, (((1,), (1,)), ((), ())),
        precision=EXACT, preferred_element_type=F32,
    )
    for i in range(1, parts):
        stat_copy(i, t).start()
    for i in range(1, parts):
        stat_copy(i, flip(t, i)).wait_recv()
    total = jnp.sum(stats[...], axis=0)
    column = lax.dot_general(
        total, jnp.full((8, 128), 0.125, F32), (((0,), (0,)), ((), ())),
        precision=EXACT, preferred_element_type=F32,
    )
    scale = lax.rsqrt(column[:, 0:1] / full + EPSILON)
    out[...] = (combined * scale * post[...]).astype(BF16)

    for j in range(levels):

        @pl.when((z >= j) & (z < levels - 1))
        def _():
            token_copy(j, True).wait_send()

        @pl.when((z <= j) & (z > 0))
        def _():
            token_copy(j, False).wait_send()

    for j in range(1, levels):
        sum_copy(j, z).wait_send()
    for i in range(1, parts):
        gain_copy(i, t).wait_send()
        stat_copy(i, t).wait_send()
    for j in range(levels):
        for d in range(1, groups):
            row_copy(j, d, e).wait_send()
            back_copy(j, flip(e, d), e).wait_send()
        for k in range(groups):
            core_copy(j, k, c).wait_send()
    for k in range(groups):
        half_copy(k).wait_send()


def local_fused(tokens, pre_gain, expert_gate, expert_up, expert_down, routes, route_weights, post_gain):
    groups, parts = lax.axis_size("ep"), lax.axis_size("tp")
    rows, width = tokens.shape
    _, features, units = expert_gate.shape
    levels = parts // CORES
    cap = 3 * rows // groups
    vmem = pl.BlockSpec(memory_space=pltpu.VMEM)
    anywhere = pl.BlockSpec(memory_space=pl.ANY)
    dma = pltpu.SemaphoreType.DMA
    block = (levels, groups, cap, width)
    by_source = (groups, levels, cap, width)
    return pl.pallas_call(
        functools.partial(fused, groups, parts),
        out_shape=jax.ShapeDtypeStruct((rows, width), BF16),
        in_specs=[vmem] * 4 + [anywhere] * 3 + [vmem],
        out_specs=vmem,
        scratch_shapes=[
            pltpu.VMEM((levels, rows, width), BF16),
            pltpu.VMEM((parts, 1, width), F32),
            pltpu.VMEM((groups, cap, rows), BF16),
            pltpu.VMEM((groups * cap, rows), F32),
            pltpu.VMEM((rows, groups * cap), BF16),
            pltpu.VMEM((rows, groups * cap), BF16),
            pltpu.VMEM(block, BF16),
            pltpu.VMEM((parts, groups, cap, width), BF16),
            pltpu.VMEM((groups, cap, 128), F32),
            pltpu.VMEM((features, units), BF16),
            pltpu.VMEM((features, units), BF16),
            pltpu.VMEM((units, features), BF16),
            pltpu.VMEM((groups, cap, units), F32),
            pltpu.VMEM((groups, cap, units), F32),
            pltpu.VMEM((cap, units), BF16),
            pltpu.VMEM(by_source, BF16),
            pltpu.VMEM(by_source, F32),
            pltpu.VMEM(by_source, BF16),
            pltpu.VMEM(by_source, BF16),
            pltpu.VMEM(block, BF16),
            pltpu.VMEM((levels, rows, width), BF16),
            pltpu.VMEM((levels, rows, width), BF16),
            pltpu.VMEM((parts, 8, rows), F32),
            dma((3,)),
            dma((levels, 2)), dma((levels,)),
            dma((parts,)), dma((parts,)),
            dma((levels, groups)), dma((levels, groups)),
            dma((levels, groups)), dma((levels, groups)),
            dma((groups,)), dma((groups,)),
            dma((groups, levels)), dma((levels, groups)),
            dma((levels,)), dma((levels,)),
            dma((parts,)), dma((parts,)),
        ],
        compiler_params=pltpu.CompilerParams(
            collective_id=0, has_side_effects=True, vmem_limit_bytes=60 * 1024 * 1024
        ),
    )(
        tokens, pre_gain.reshape(1, width), routes.T, route_weights.T,
        expert_gate, expert_up, expert_down, post_gain.reshape(1, width),
    )


def power_of_two(count):
    return count & (count - 1) == 0


def plan(mesh):
    def choose(*args):
        tokens, gate = args[0], args[2]
        groups, parts = mesh.shape["ep"], mesh.shape["tp"]
        rows, width = tokens.shape
        fits = (
            gate.shape[0] == 1
            and power_of_two(groups)
            and power_of_two(parts)
            and 2 <= groups <= 8
            and parts >= 2 * CORES
            and width % 128 == 0
            and rows % 128 == 0
            and (3 * rows // groups) % 16 == 0
            and (3 * rows) % 128 == 0
            and gate.shape[2] % 128 == 0
        )
        return (local_fused if fits else local)(*args)

    return choose


def solution(mesh):
    placed = (
        P("ep", "tp"),
        P("tp"),
        P("ep", None, "tp"),
        P("ep", None, "tp"),
        P("ep", "tp", None),
        P("ep", None),
        P("ep", None),
        P("tp"),
    )
    return jax.shard_map(
        plan(mesh), mesh=mesh, in_specs=placed, out_specs=P("ep", "tp"), check_vma=False
    )
```

profile of v0, /device:TPU:0, one launch (start us, length us, event | category | flops | bytes accessed | tf_op | source)
XLA Modules:
  0.0 67.0 jit_solution(1132376372315102964)
XLA Ops:
  0.0 65.4 %shard_map.82 = bf16[256,256]{1,0:T(8,128)(2,1)} custom-call(bf16[256,256]{1,0:T(8,128)(2,1)} %tok.1, f32[1,256]{1,0:T(1,128)} %bitcast.6, s32[2,256]{1,0:T(2,128)} %bitcast.4, f32[2,256]{1,0:T(2,128)} %bitcast.5, bf16[1,2048,1024]{2,1,0:T(8,128)(2,1)} %gate_hbm.1, bf16[1,2048,1024]{2,1,0:T(8,128)(2,1)} %up_hbm.1, bf16[1,1024,2048]{2,1,0:T(8,128)(2,1)} %down_hbm.1, ...), custom_call_target="tpu_custom_call" | custom-call | tf_op jit(solution)/shard_map/pallas_call | solution.py:381
  65.4 1.6 %copy.10 = bf16[256,256]{1,0:T(8,128)(2,1)} copy(bf16[256,256]{1,0:T(8,128)(2,1)} %shard_map.82) | data formatting | bytes 262144
where the time goes:
time: 67.1 us; the launch traced here: 67 us
  Pallas kernels  65.4 us (97%)
  local copies, waits for them, and re-layouts  1.57 us (2%)
    pallas_call x1, Pallas kernels, local_fused(): pl.pallas_call(functools.partial(fused, groups, parts), out_shape=jax.Sha...  65.4 us
    unnamed x1, local copies, waits for them, and re-layouts  1.57 us

commit v1 on v0

v1 whole, which is shorter than its diff:
```python
import functools

import jax
import jax.numpy as jnp
from jax import lax
from jax.experimental import pallas as pl
from jax.experimental.pallas import tpu as pltpu
from jax.sharding import PartitionSpec as P

EPSILON = 1e-06


def local(tokens, pre_gain, expert_gate, expert_up, expert_down, routes, route_weights, post_gain):
    local_experts = expert_gate.shape[0]
    groups = lax.axis_size("ep")
    experts_all = local_experts * groups
    tok_rows, part_width = tokens.shape
    full_width = part_width * lax.axis_size("tp")
    capacity = 3 * tok_rows // experts_all
    values = tokens.astype(jnp.float32)
    input_sq = lax.psum(jnp.sum(values * values, axis=-1), "tp")
    normed = (
        values * lax.rsqrt(input_sq / full_width + EPSILON)[:, None] * pre_gain[None, :]
    ).astype(jnp.bfloat16)
    onehot = (routes[:, :, None] == jnp.arange(experts_all, dtype=jnp.int32)).astype(jnp.int32)
    onehot = onehot.reshape(tok_rows * 2, experts_all)
    earlier = jnp.cumsum(onehot, axis=0) - onehot
    slots = jnp.sum(earlier * onehot, axis=-1).reshape(tok_rows, 2)
    positions = routes * capacity + slots
    places = jnp.arange(experts_all * capacity, dtype=jnp.int32)
    first_pick = (places[:, None] == positions[None, :, 0]).astype(jnp.bfloat16)
    second_pick = (places[:, None] == positions[None, :, 1]).astype(jnp.bfloat16)
    dispatch = first_pick + second_pick
    outgoing = jnp.dot(dispatch, normed, preferred_element_type=jnp.float32).astype(jnp.bfloat16)
    arrived = lax.all_to_all(outgoing, "ep", split_axis=0, concat_axis=0, tiled=True)
    fragment = lax.all_gather(arrived, "tp", axis=1, tiled=True)
    count = fragment.shape[1]
    grouped = fragment.reshape(groups, local_experts, capacity, count)
    gate_pre = jnp.einsum(
        "secw,ewf->secf", grouped, expert_gate, preferred_element_type=jnp.float32
    )
    up_pre = jnp.einsum("secw,ewf->secf", grouped, expert_up, preferred_element_type=jnp.float32)
    hidden = (jax.nn.silu(gate_pre) * up_pre).astype(jnp.bfloat16)
    product = jnp.einsum("secf,efd->dsec", hidden, expert_down, preferred_element_type=jnp.float32)
    summed = lax.psum_scatter(
        product.reshape(lax.axis_size("tp") * part_width, groups * local_experts * capacity).astype(
            jnp.bfloat16
        ),
        "tp",
        scatter_dimension=0,
        tiled=True,
    )
    returned = lax.all_to_all(summed, "ep", split_axis=1, concat_axis=1, tiled=True)
    contract = (((0,), (1,)), ((), ()))
    first_out = lax.dot_general(first_pick, returned, contract, preferred_element_type=jnp.float32)
    second_out = lax.dot_general(
        second_pick, returned, contract, preferred_element_type=jnp.float32
    )
    combined = route_weights[:, 0:1] * first_out + route_weights[:, 1:2] * second_out
    output_sq = lax.psum(jnp.sum(combined * combined, axis=-1), "tp")
    scaled = combined * lax.rsqrt(output_sq / full_width + EPSILON)[:, None] * post_gain[None, :]
    return scaled.astype(jnp.bfloat16)


CORES = 2
PIECES = 2
F32 = jnp.float32
BF16 = jnp.bfloat16
MESH = pl.DeviceIdType.MESH


def flip(index, bits):
    place = 1
    while place <= bits:
        if bits & place:
            index = index + place - 2 * place * lax.rem(lax.div(index, place), 2)
        place *= 2
    return index


def flip_traced(index, bits, size):
    total, place = 0, 1
    while place < size:
        total = total + place * lax.rem(lax.div(index, place) + lax.div(bits, place), 2)
        place *= 2
    return total


def fused(
    groups, parts, tok, gain, route, weight, gate_hbm, up_hbm, down_hbm, post, out,
    zbuf, fbuf, gains, route1, weight1, disp, mix, x, xnear, xfar, squares,
    gate, up, down, acc_gate, acc_up, hidden, half, half_in, own, mine, theirs,
    back_near, back_far, csend, cin, zsend, zin, stats,
    wsem, zs, zr, gs, gr, us, ur, rs, rr, ns, nr, bs, br, fs, fr, ds, dr,
    qs, qr, hs, hr, cs, cr, ts, tr, ps, pr,
):
    t, e = lax.axis_index("tp"), lax.axis_index("ep")
    z, c = lax.div(t, CORES), lax.rem(t, CORES)
    levels = parts // CORES
    rows, width = tok.shape
    cap = xnear.shape[1]
    full = parts * width
    e1, e2, e3 = flip(e, 1), flip(e, 2), flip(e, 3)
    first_hop = (1 - c) * e1 + c * e2
    second_hop = (1 - c) * e2 + c * e1

    barrier = pltpu.get_barrier_semaphore()
    for i in range(1, parts):
        pl.semaphore_signal(barrier, inc=1, device_id={"tp": flip(t, i)}, device_id_type=MESH)
    for d in (1, 2):
        pl.semaphore_signal(barrier, inc=1, device_id={"ep": flip(e, d)}, device_id_type=MESH)

    loads = [
        pltpu.make_async_copy(gate_hbm.at[0], gate, wsem.at[0]),
        pltpu.make_async_copy(up_hbm.at[0], up, wsem.at[1]),
        pltpu.make_async_copy(down_hbm.at[0], down, wsem.at[2]),
    ]
    for load in loads:
        load.start()

    def remote(src, dst, send, recv, **device):
        return pltpu.make_async_remote_copy(
            src_ref=src, dst_ref=dst, send_sem=send, recv_sem=recv,
            device_id=device, device_id_type=MESH,
        )

    def piece_of(ref, level, h):
        return ref.at[level, pl.ds(h * (rows // PIECES), rows // PIECES)]

    def token_copy(level, h, up):
        step = 1 if up else -1
        source = piece_of(zbuf, level, h)
        return remote(source, source, zs.at[level, h, int(up)], zr.at[level, h], tp=t + step * CORES)

    def raw_copy(level, h):
        return remote(
            piece_of(zbuf, level, h), piece_of(fbuf, level, h),
            rs.at[level, h], rr.at[level, h], ep=first_hop,
        )

    def relay(k):
        for h in range(PIECES):

            @pl.when(z >= k)
            def _():
                if k:
                    token_copy(z - k, h, True).wait_recv()

                @pl.when(z < levels - 1)
                def _():
                    token_copy(z - k, h, True).start()

            @pl.when(z + k < levels)
            def _():
                if k:
                    token_copy(z + k, h, False).wait_recv()

                @pl.when(z > 0)
                def _():
                    token_copy(z + k, h, False).start()

            raw_copy(flip(z, k), h).start()

    def gain_copy(i, part):
        return remote(gain, gains.at[part], gs.at[i], gr.at[part], tp=flip(t, i))

    def route_copies():
        return (
            remote(route, route1, us.at[0], ur.at[0], ep=first_hop),
            remote(weight, weight1, us.at[1], ur.at[1], ep=first_hop),
        )

    def near_copy(level, source):
        return remote(
            xnear.at[level], x.at[level * CORES + c, source], ns.at[level], nr.at[level],
            ep=second_hop,
        )

    def far_copy(level, source):
        return remote(
            xfar.at[level], x.at[level * CORES + c, source], bs.at[level], br.at[level],
            ep=second_hop,
        )

    def core_copy(level, source, core):
        slot = x.at[level * CORES + core, source]
        return remote(slot, slot, fs.at[level, source], fr.at[level, source], tp=z * CORES + 1 - c)

    def half_copy(level, kind):
        span = pl.ds(groups - 1, 1) if kind else pl.ds(0, groups - 1)
        return remote(
            half.at[level, span], half_in.at[level, span],
            ds.at[level, kind], dr.at[level, kind], tp=z * CORES + 1 - c,
        )

    def back_near_copy(level):
        return remote(
            back_near.at[level], mine.at[level, 1], qs.at[level], qr.at[level], ep=second_hop
        )

    def back_far_copy(level):
        return remote(
            back_far.at[level], theirs.at[level, 1], hs.at[level], hr.at[level], ep=second_hop
        )

    def mixed_copy(level):
        return remote(csend.at[level], cin.at[level], cs.at[level], cr.at[level], ep=first_hop)

    def sum_copy(j):
        bits = 2 if j == 2 else 1
        return remote(
            zsend.at[j], zin.at[j], ts.at[j], tr.at[j], tp=flip(z, bits) * CORES + c
        )

    def stat_copy(i, part):
        return remote(stats.at[t], stats.at[part], ps.at[i], pr.at[part], tp=flip(t, i))

    def plan_rows(which, r, w):
        first, second = r[0:1], r[1:2]
        lanes = lax.broadcasted_iota(jnp.int32, (8, rows), 0)
        names = jnp.where(lanes == 0, e, jnp.where(lanes == 1, second_hop, -1))
        member = jnp.where((names == first) | (names == second), 1.0, 0.0)
        before = jnp.where(
            lax.broadcasted_iota(jnp.int32, (rows, rows), 0)
            < lax.broadcasted_iota(jnp.int32, (rows, rows), 1),
            1.0, 0.0,
        )
        slots = jnp.dot(member.astype(BF16), before.astype(BF16), preferred_element_type=F32)
        slots = jnp.where(member > 0.5, slots, -1.0).astype(jnp.int32)
        lines = lax.broadcasted_iota(jnp.int32, (cap, rows), 0)
        spread = []
        for k, name in enumerate((e, second_hop)):
            hit = lines == slots[k : k + 1]
            disp[which, k * cap : (k + 1) * cap, :] = jnp.where(hit, 1.0, 0.0).astype(BF16)
            chosen = jnp.where(first == name, w[0:1], w[1:2])
            spread.append(jnp.where(hit, chosen, 0.0))
        return spread

    def plan_mix(which, spread):
        for k in range(2):
            mix[which, :, k * cap : (k + 1) * cap] = spread[k].T.astype(BF16)

    acc_gate[...] = jnp.zeros_like(acc_gate)
    acc_up[...] = jnp.zeros_like(acc_up)
    squares[...] = jnp.zeros_like(squares)
    zbuf[z] = tok[...]
    gains[t] = gain[...]
    own_spread = plan_rows(0, route[...], weight[...])

    pl.semaphore_wait(barrier, parts + 1)
    for copy in route_copies():
        copy.start()
    relay(0)

    def pick_own(j):
        level = flip(z, j)
        picked = jnp.dot(disp[0], zbuf[level], preferred_element_type=F32).astype(BF16)
        x[level * CORES + c, e] = picked[:cap]
        core_copy(level, e, c).start()
        xnear[level] = picked[cap:]
        near_copy(level, e).start()

    def pick_far(j):
        level = flip(z, j)
        for h in range(PIECES):
            raw_copy(level, h).wait_recv()
        picked = jnp.dot(disp[1], fbuf[level], preferred_element_type=F32).astype(BF16)
        xfar[level] = picked[cap:]
        far_copy(level, first_hop).start()
        x[level * CORES + c, first_hop] = picked[:cap]
        core_copy(level, first_hop, c).start()

    def pass_far(j):
        level = flip(z, j)
        far_copy(level, e3).wait_recv()
        core_copy(level, e3, c).start()

    def pass_near(j):
        level = flip(z, j)
        near_copy(level, second_hop).wait_recv()
        core_copy(level, second_hop, c).start()

    def piece(part, source):
        values = x[part, source].astype(F32)
        square = values * values
        total = square[:, 0:128]
        for lane in range(128, width, 128):
            total = total + square[:, lane : lane + 128]
        scaled = (values * gains[part]).astype(BF16)
        depth = pl.ds(pl.multiple_of(part * width, 128), width)
        return (
            total,
            jnp.dot(scaled, gate[depth, :], preferred_element_type=F32),
            jnp.dot(scaled, up[depth, :], preferred_element_type=F32),
        )

    def level_sum(level, role):
        source = flip_traced(e, role, groups)
        core_copy(level, source, 1 - c).wait_recv()
        found = (squares[role], acc_gate[role], acc_up[role])
        for core in range(CORES):
            found = [p + q for p, q in zip(piece(level * CORES + core, source), found)]
        return found

    def collect(j, low, high):
        def body(role, carry):
            level = flip_traced(z, j - lax.div(role + 1, 2), levels)
            squares[role], acc_gate[role], acc_up[role] = level_sum(level, role)
            return carry

        lax.fori_loop(low, high, body, 0)

    def activate(low, high):
        def body(role, carry):
            total, gate_part, up_part = level_sum(flip(z, levels - 1), role)
            scale = lax.rsqrt(jnp.sum(total, axis=1, keepdims=True) / full + EPSILON)
            gate_part = gate_part * scale
            share = 0.5 + 0.5 * jnp.tanh(0.5 * gate_part)
            hidden[role] = (gate_part * share * (up_part * scale)).astype(BF16)
            return carry

        lax.fori_loop(low, high, body, 0)

    def descend(j, kind):
        level = flip(z, j)
        span = slice(groups - 1, groups) if kind else slice(0, groups - 1)
        count = 1 if kind else groups - 1
        left = hidden[span].reshape(count * cap, hidden.shape[2])

        def block(core):
            columns = pl.ds(pl.multiple_of((level * CORES + core) * width, 128), width)
            return jnp.dot(left, down[:, columns], preferred_element_type=F32)

        other, this = block(1 - c), block(c)
        half[level, span] = other.reshape(count, cap, width).astype(BF16)
        own[level, span] = this.reshape(count, cap, width)
        half_copy(level, kind).start()

    def summed(level, role):
        return (own[level, role] + half_in[level, role].astype(F32)).astype(BF16)

    def finish_far(j):
        level = flip(z, j)
        half_copy(level, 1).wait_recv()
        back_far[level] = summed(level, groups - 1)
        back_far_copy(level).start()

    def finish_near(j):
        level = flip(z, j)
        half_copy(level, 0).wait_recv()
        back_near[level] = summed(level, 2 - c)
        back_near_copy(level).start()
        theirs[level, 0] = summed(level, 1 + c)
        mine[level, 0] = summed(level, 0)

    def combine(which, results):
        return jnp.dot(
            mix[which], results.reshape(2 * cap, width), preferred_element_type=F32
        )

    def hand_over(j):
        level = flip(z, j)
        back_far_copy(level).wait_recv()
        csend[level] = combine(1, theirs[level]).astype(BF16)
        mixed_copy(level).start()

    def settle(j):
        level = flip(z, j)
        back_near_copy(level).wait_recv()
        combined = combine(0, mine[level])
        mixed_copy(level).wait_recv()
        combined = combined + cin[level].astype(F32)
        for source in {3: (), 2: (3,), 1: (), 0: (2, 1)}[j]:
            sum_copy(source).wait_recv()
            combined = combined + zin[source].astype(F32)
        if j:
            zsend[j] = combined.astype(BF16)
            sum_copy(j).start()
        return combined

    pick_own(0)
    for i in range(1, parts):
        gain_copy(i, t).start()
    for copy in route_copies():
        copy.wait_recv()
    far_spread = plan_rows(1, route1[...], weight1[...])
    plan_mix(0, own_spread)
    plan_mix(1, far_spread)
    for i in range(1, parts):
        gain_copy(i, flip(t, i)).wait_recv()
    loads[0].wait()
    loads[1].wait()
    collect(0, 0, 1)
    for j in range(1, levels):
        relay(j)
        pick_far(j - 1)
        pick_own(j)
        pass_near(j - 1)
        if j > 1:
            pass_far(j - 2)
        collect(j, 1 if j == levels - 1 else 0, 4 if j > 1 else 3)
        if j == levels - 1:
            activate(0, 1)
    pick_far(levels - 1)
    pass_near(levels - 1)
    pass_far(levels - 2)
    collect(levels, 3, 4)
    activate(1, 3)
    pass_far(levels - 1)
    activate(3, 4)
    loads[2].wait()
    descend(3, 1)
    descend(2, 1)
    descend(1, 1)
    finish_far(3)
    descend(0, 1)
    finish_far(2)
    descend(3, 0)
    finish_far(1)
    descend(2, 0)
    finish_far(0)
    finish_near(3)
    descend(1, 0)
    finish_near(2)
    hand_over(3)
    descend(0, 0)
    finish_near(1)
    hand_over(2)
    finish_near(0)
    hand_over(1)
    settle(3)
    hand_over(0)
    for j in range(levels - 2, -1, -1):
        combined = settle(j)

    square = combined * combined
    folded = square[:, 0:128]
    for lane in range(128, width, 128):
        folded = folded + square[:, lane : lane + 128]
    stats[t] = jnp.sum(folded.T.reshape(16, 8, rows), axis=0)
    for i in range(1, parts):
        stat_copy(i, t).start()
    for i in range(1, parts):
        stat_copy(i, flip(t, i)).wait_recv()
    total = jnp.sum(stats[...], axis=0)
    high = total.astype(BF16)
    ones = jnp.ones((8, 128), BF16)
    column = sum(
        lax.dot_general(v, ones, (((0,), (0,)), ((), ())), preferred_element_type=F32)
        for v in (high, (total - high.astype(F32)).astype(BF16))
    )
    scale = lax.rsqrt(column[:, 0:1] / full + EPSILON)
    out[...] = (combined * scale * post[...]).astype(BF16)

    for j in range(levels):

        for h in range(PIECES):

            @pl.when((z >= j) & (z < levels - 1))
            def _():
                token_copy(j, h, True).wait_send()

            @pl.when((z <= j) & (z > 0))
            def _():
                token_copy(j, h, False).wait_send()

            raw_copy(j, h).wait_send()

    for copy in route_copies():
        copy.wait_send()
    for j in range(1, levels):
        sum_copy(j).wait_send()
    for i in range(1, parts):
        gain_copy(i, t).wait_send()
        stat_copy(i, t).wait_send()
    for j in range(levels):
        near_copy(j, e).wait_send()
        far_copy(j, first_hop).wait_send()
        for source in range(groups):
            core_copy(j, source, c).wait_send()
        half_copy(j, 0).wait_send()
        half_copy(j, 1).wait_send()
        back_near_copy(j).wait_send()
        back_far_copy(j).wait_send()
        mixed_copy(j).wait_send()


def local_fused(tokens, pre_gain, expert_gate, expert_up, expert_down, routes, route_weights, post_gain):
    groups, parts = lax.axis_size("ep"), lax.axis_size("tp")
    rows, width = tokens.shape
    _, features, units = expert_gate.shape
    levels = parts // CORES
    cap = 3 * rows // groups
    vmem = pl.BlockSpec(memory_space=pltpu.VMEM)
    anywhere = pl.BlockSpec(memory_space=pl.ANY)
    dma = pltpu.SemaphoreType.DMA
    tok_block = pltpu.VMEM((levels, rows, width), BF16)
    row_block = pltpu.VMEM((levels, cap, width), BF16)
    block = (levels, groups, cap, width)
    return pl.pallas_call(
        functools.partial(fused, groups, parts),
        out_shape=jax.ShapeDtypeStruct((rows, width), BF16),
        in_specs=[vmem] * 4 + [anywhere] * 3 + [vmem],
        out_specs=vmem,
        scratch_shapes=[
            tok_block,
            tok_block,
            pltpu.VMEM((parts, 1, width), F32),
            pltpu.VMEM((2, rows), jnp.int32),
            pltpu.VMEM((2, rows), F32),
            pltpu.VMEM((2, 2 * cap, rows), BF16),
            pltpu.VMEM((2, rows, 2 * cap), BF16),
            pltpu.VMEM((parts, groups, cap, width), BF16),
            row_block,
            row_block,
            pltpu.VMEM((groups, cap, 128), F32),
            pltpu.VMEM((features, units), BF16),
            pltpu.VMEM((features, units), BF16),
            pltpu.VMEM((units, features), BF16),
            pltpu.VMEM((groups, cap, units), F32),
            pltpu.VMEM((groups, cap, units), F32),
            pltpu.VMEM((groups, cap, units), BF16),
            pltpu.VMEM(block, BF16),
            pltpu.VMEM(block, BF16),
            pltpu.VMEM(block, F32),
            pltpu.VMEM((levels, 2, cap, width), BF16),
            pltpu.VMEM((levels, 2, cap, width), BF16),
            row_block,
            row_block,
            tok_block,
            tok_block,
            tok_block,
            tok_block,
            pltpu.VMEM((parts, 8, rows), F32),
            dma((3,)),
            dma((levels, PIECES, 2)), dma((levels, PIECES)),
            dma((parts,)), dma((parts,)),
            dma((2,)), dma((2,)),
            dma((levels, PIECES)), dma((levels, PIECES)),
            dma((levels,)), dma((levels,)),
            dma((levels,)), dma((levels,)),
            dma((levels, groups)), dma((levels, groups)),
            dma((levels, 2)), dma((levels, 2)),
            dma((levels,)), dma((levels,)),
            dma((levels,)), dma((levels,)),
            dma((levels,)), dma((levels,)),
            dma((levels,)), dma((levels,)),
            dma((parts,)), dma((parts,)),
        ],
        compiler_params=pltpu.CompilerParams(
            collective_id=0, has_side_effects=True, vmem_limit_bytes=60 * 1024 * 1024
        ),
    )(
        tokens, pre_gain.reshape(1, width), routes.T, route_weights.T,
        expert_gate, expert_up, expert_down, post_gain.reshape(1, width),
    )


def plan(mesh):
    def choose(*args):
        tokens, gate = args[0], args[2]
        groups, parts = mesh.shape["ep"], mesh.shape["tp"]
        rows, width = tokens.shape
        fits = (
            gate.shape[0] == 1
            and groups == 4
            and parts == 4 * CORES
            and width % 128 == 0
            and rows % 128 == 0
            and (3 * rows // groups) % 64 == 0
            and gate.shape[2] % 128 == 0
        )
        return (local_fused if fits else local)(*args)

    return choose


def solution(mesh):
    placed = (
        P("ep", "tp"),
        P("tp"),
        P("ep", None, "tp"),
        P("ep", None, "tp"),
        P("ep", "tp", None),
        P("ep", None),
        P("ep", None),
        P("tp"),
    )
    return jax.shard_map(
        plan(mesh), mesh=mesh, in_specs=placed, out_specs=P("ep", "tp"), check_vma=False
    )
```

time: 67.1 us -> 63 us (0.939)
  Pallas kernels: 65.4 us -> 61.3 us
    pallas_call x1, Pallas kernels: 65.4 us -> 61.3 us  [local_fused(): pl.pallas_call(functools.partial(fused, groups, parts), out_shape=jax.Sha...]
where the time goes in v1:
time: 63 us; the launch traced here: 62.9 us
  Pallas kernels  61.3 us (97%)
  local copies, waits for them, and re-layouts  1.57 us (2%)
    pallas_call x1, Pallas kernels, local_fused(): pl.pallas_call(functools.partial(fused, groups, parts), out_shape=jax.Sha...  61.3 us
    unnamed x1, local copies, waits for them, and re-layouts  1.57 us

profile of v1, /device:TPU:0, one launch (start us, length us, event | category | flops | bytes accessed | tf_op | source)
XLA Modules:
  0.0 62.9 jit_solution(10220104374602183656)
XLA Ops:
  0.0 61.3 %shard_map.82 = bf16[256,256]{1,0:T(8,128)(2,1)} custom-call(bf16[256,256]{1,0:T(8,128)(2,1)} %tok.1, f32[1,256]{1,0:T(1,128)} %bitcast.6, s32[2,256]{1,0:T(2,128)} %bitcast.4, f32[2,256]{1,0:T(2,128)} %bitcast.5, bf16[1,2048,1024]{2,1,0:T(8,128)(2,1)} %gate_hbm.1, bf16[1,2048,1024]{2,1,0:T(8,128)(2,1)} %up_hbm.1, bf16[1,1024,2048]{2,1,0:T(8,128)(2,1)} %down_hbm.1, ...), custom_call_target="tpu_custom_call" | custom-call | tf_op jit(solution)/shard_map/pallas_call | solution.py:500
  61.3 1.6 %copy.10 = bf16[256,256]{1,0:T(8,128)(2,1)} copy(bf16[256,256]{1,0:T(8,128)(2,1)} %shard_map.82) | data formatting | bytes 262144

commit v2 on v0

v2 whole, which is shorter than its diff:
```python
import functools

import jax
import jax.numpy as jnp
from jax import lax
from jax.experimental import pallas as pl
from jax.experimental.pallas import tpu as pltpu
from jax.sharding import PartitionSpec as P

EPSILON = 1e-06


def local(tokens, pre_gain, expert_gate, expert_up, expert_down, routes, route_weights, post_gain):
    local_experts = expert_gate.shape[0]
    groups = lax.axis_size("ep")
    experts_all = local_experts * groups
    tok_rows, part_width = tokens.shape
    full_width = part_width * lax.axis_size("tp")
    capacity = 3 * tok_rows // experts_all
    values = tokens.astype(jnp.float32)
    input_sq = lax.psum(jnp.sum(values * values, axis=-1), "tp")
    normed = (
        values * lax.rsqrt(input_sq / full_width + EPSILON)[:, None] * pre_gain[None, :]
    ).astype(jnp.bfloat16)
    onehot = (routes[:, :, None] == jnp.arange(experts_all, dtype=jnp.int32)).astype(jnp.int32)
    onehot = onehot.reshape(tok_rows * 2, experts_all)
    earlier = jnp.cumsum(onehot, axis=0) - onehot
    slots = jnp.sum(earlier * onehot, axis=-1).reshape(tok_rows, 2)
    positions = routes * capacity + slots
    places = jnp.arange(experts_all * capacity, dtype=jnp.int32)
    first_pick = (places[:, None] == positions[None, :, 0]).astype(jnp.bfloat16)
    second_pick = (places[:, None] == positions[None, :, 1]).astype(jnp.bfloat16)
    dispatch = first_pick + second_pick
    outgoing = jnp.dot(dispatch, normed, preferred_element_type=jnp.float32).astype(jnp.bfloat16)
    arrived = lax.all_to_all(outgoing, "ep", split_axis=0, concat_axis=0, tiled=True)
    fragment = lax.all_gather(arrived, "tp", axis=1, tiled=True)
    count = fragment.shape[1]
    grouped = fragment.reshape(groups, local_experts, capacity, count)
    gate_pre = jnp.einsum(
        "secw,ewf->secf", grouped, expert_gate, preferred_element_type=jnp.float32
    )
    up_pre = jnp.einsum("secw,ewf->secf", grouped, expert_up, preferred_element_type=jnp.float32)
    hidden = (jax.nn.silu(gate_pre) * up_pre).astype(jnp.bfloat16)
    product = jnp.einsum("secf,efd->dsec", hidden, expert_down, preferred_element_type=jnp.float32)
    summed = lax.psum_scatter(
        product.reshape(lax.axis_size("tp") * part_width, groups * local_experts * capacity).astype(
            jnp.bfloat16
        ),
        "tp",
        scatter_dimension=0,
        tiled=True,
    )
    returned = lax.all_to_all(summed, "ep", split_axis=1, concat_axis=1, tiled=True)
    contract = (((0,), (1,)), ((), ()))
    first_out = lax.dot_general(first_pick, returned, contract, preferred_element_type=jnp.float32)
    second_out = lax.dot_general(
        second_pick, returned, contract, preferred_element_type=jnp.float32
    )
    combined = route_weights[:, 0:1] * first_out + route_weights[:, 1:2] * second_out
    output_sq = lax.psum(jnp.sum(combined * combined, axis=-1), "tp")
    scaled = combined * lax.rsqrt(output_sq / full_width + EPSILON)[:, None] * post_gain[None, :]
    return scaled.astype(jnp.bfloat16)


CORES = 2
PIECES = 4
HALVES = 2
F32 = jnp.float32
BF16 = jnp.bfloat16
MESH = pl.DeviceIdType.MESH


def flip(index, bits):
    place = 1
    while place <= bits:
        if bits & place:
            index = index + place - 2 * place * lax.rem(lax.div(index, place), 2)
        place *= 2
    return index


BATCHES = (
    ((0, 0),), ((0, 1),), ((1, 0), (2, 0)), ((3, 0), (0, 2)), ((1, 1), (2, 1)), ((3, 1), (0, 3)),
    ((1, 2), (2, 2)), ((3, 2),), ((1, 3),), ((2, 3),), ((3, 3),),
)


def fused(
    groups, parts, tok, gain, route_in, weight_in, gate_hbm, up_hbm, down_hbm, post_in, out,
    zbuf, gains, route, weight, post, disp, mix, x, xsend, squares,
    gate, up, down, acc_gate, acc_up, hidden, half, half_in, own, back, ret,
    hand, hand_in, zsend, zin, stats,
    isem, wsem, zs, zr, gs, gr, ns, nr, fs, fr, ds, dr, qs, qr, hs, hr, ts, tr, ps, pr,
):
    t, e = lax.axis_index("tp"), lax.axis_index("ep")
    z, c = lax.div(t, CORES), lax.rem(t, CORES)
    levels = parts // CORES
    rows, width = zbuf.shape[1:]
    cap = xsend.shape[2]
    full = parts * width
    around = [flip(e, role) if role else e for role in range(groups)]
    batch_of = {unit: k for k, batch in enumerate(BATCHES) for unit in batch}

    barrier = pltpu.get_barrier_semaphore()
    for i in range(1, parts):
        pl.semaphore_signal(barrier, inc=1, device_id={"tp": flip(t, i)}, device_id_type=MESH)
    for d in range(1, groups):
        pl.semaphore_signal(barrier, inc=1, device_id={"ep": flip(e, d)}, device_id_type=MESH)

    inputs = [
        pltpu.make_async_copy(route_in, route, isem.at[0]),
        pltpu.make_async_copy(weight_in, weight, isem.at[1]),
        pltpu.make_async_copy(tok, zbuf.at[z], isem.at[2]),
        pltpu.make_async_copy(gain, gains.at[t], isem.at[3]),
        pltpu.make_async_copy(post_in, post, isem.at[4]),
    ]
    for copy in inputs:
        copy.start()
    loads = [
        pltpu.make_async_copy(gate_hbm.at[0], gate, wsem.at[0]),
        pltpu.make_async_copy(up_hbm.at[0], up, wsem.at[1]),
        pltpu.make_async_copy(down_hbm.at[0], down, wsem.at[2]),
    ]
    for load in loads:
        load.start()

    def remote(src, dst, send, recv, **device):
        return pltpu.make_async_remote_copy(
            src_ref=src, dst_ref=dst, send_sem=send, recv_sem=recv,
            device_id=device, device_id_type=MESH,
        )

    def piece_of(ref, level, h, count):
        return ref.at[level, pl.ds(h * (rows // count), rows // count)]

    def token_copy(level, h, up):
        step = 1 if up else -1
        source = piece_of(zbuf, level, h, PIECES)
        return remote(source, source, zs.at[int(up)], zr.at[level, h], tp=t + step * CORES)

    def relay(k, h):
        @pl.when(z >= k)
        def _():
            if k:
                token_copy(z - k, h, True).wait_recv()

            @pl.when(z < levels - 1)
            def _():
                token_copy(z - k, h, True).start()

        @pl.when(z + k < levels)
        def _():
            if k:
                token_copy(z + k, h, False).wait_recv()

            @pl.when(z > 0)
            def _():
                token_copy(z + k, h, False).start()

    def gain_copy(i, part):
        return remote(gains.at[part], gains.at[part], gs, gr, tp=flip(t, i))

    def row_copy(level, role, source):
        return remote(
            xsend.at[level, role - 1], x.at[level * CORES + c, source],
            ns, nr.at[level, role - 1], ep=around[role],
        )

    def core_copy(j, role):
        slot = x.at[flip(z, j) * CORES + c, around[role]]
        return remote(slot, slot, fs, fr.at[batch_of[role, j]], tp=z * CORES + 1 - c)

    def half_copy(level, kind):
        span = pl.ds(groups - 1, 1) if kind else pl.ds(0, groups - 1)
        return remote(
            half.at[level, span], half_in.at[level, span],
            ds, dr.at[level, kind], tp=z * CORES + 1 - c,
        )

    def back_copy(level, role):
        return remote(
            back.at[level, role - 1], ret.at[level, role],
            qs, qr.at[level, role - 1], ep=around[role],
        )

    def hand_copy(kind):
        span = pl.ds(groups - 1, 1) if kind else pl.ds(0, groups - 1)
        return remote(
            hand.at[span], hand_in.at[span], hs, hr.at[kind], tp=flip(z, 1) * CORES + c
        )

    def sum_copy(j, h):
        bits = 2 if j == 2 else 1
        return remote(
            piece_of(zsend, j, h, HALVES), piece_of(zin, j, h, HALVES),
            ts, tr.at[j, h], tp=flip(z, bits) * CORES + c,
        )

    def stat_copy(i, part):
        return remote(stats.at[t], stats.at[part], ps, pr, tp=flip(t, i))

    def plan_rows():
        r, w = route[...], weight[...]
        first, second = r[0:1], r[1:2]
        lanes = lax.broadcasted_iota(jnp.int32, (8, rows), 0)
        names = jnp.full((8, rows), -1, jnp.int32)
        for role in range(groups):
            names = jnp.where(lanes == role, around[role], names)
        member = jnp.where((names == first) | (names == second), 1.0, 0.0)
        before = jnp.where(
            lax.broadcasted_iota(jnp.int32, (rows, rows), 0)
            < lax.broadcasted_iota(jnp.int32, (rows, rows), 1),
            1.0, 0.0,
        )
        slots = jnp.dot(member.astype(BF16), before.astype(BF16), preferred_element_type=F32)
        slots = jnp.where(member > 0.5, slots, -1.0).astype(jnp.int32)
        lines = lax.broadcasted_iota(jnp.int32, (cap, rows), 0)
        spread = []
        for role in range(groups):
            hit = lines == slots[role : role + 1]
            disp[role * cap : (role + 1) * cap, :] = jnp.where(hit, 1.0, 0.0).astype(BF16)
            chosen = jnp.where(first == around[role], w[0:1], w[1:2])
            spread.append(jnp.where(hit, chosen, 0.0))
        return spread

    def plan_mix(spread):
        mix[...] = jnp.concatenate(spread, axis=0).T.astype(BF16)

    for copy in inputs[:4]:
        copy.wait()
    pl.semaphore_wait(barrier, parts + groups - 2)
    for i in range(1, parts):
        gain_copy(i, t).start()
    for h in range(PIECES):
        relay(0, h)

    def pick(j):
        level = flip(z, j)
        picked = jnp.dot(disp[...], zbuf[level], preferred_element_type=F32).astype(BF16)
        for role in range(1, groups):
            xsend[level, role - 1] = picked[role * cap : (role + 1) * cap]
        x[level * CORES + c, e] = picked[:cap]
        for role in range(1, groups):
            row_copy(level, role, e).start()
        core_copy(j, 0).start()

    def pass_on(j, role):
        row_copy(flip(z, j), role, around[role]).wait_recv()
        core_copy(j, role).start()

    def level_sum(j, role):
        level, source = flip(z, j), around[role]
        total, scaled = 0.0, []
        for core in range(CORES):
            part = level * CORES + core
            values = x[part, source].astype(F32)
            square = values * values
            for lane in range(0, width, 128):
                total = total + square[:, lane : lane + 128]
            scaled.append((values * gains[part]).astype(BF16))
        left = jnp.concatenate(scaled, axis=1)
        depth = pl.ds(pl.multiple_of(level * CORES * width, CORES * 128), CORES * width)
        found = (
            total,
            jnp.dot(left, gate[depth, :], preferred_element_type=F32),
            jnp.dot(left, up[depth, :], preferred_element_type=F32),
        )
        if j:
            found = [p + ref[role] for p, ref in zip(found, (squares, acc_gate, acc_up))]
        return found

    def project(k):
        batch = BATCHES[k]
        slots = x.at[0, pl.ds(0, len(batch))]
        remote(slots, slots, fs, fr.at[k], tp=z * CORES + 1 - c).wait_recv()
        for role, j in batch:
            found = level_sum(j, role)
            if j < levels - 1:
                squares[role], acc_gate[role], acc_up[role] = found
                continue
            total, gate_part, up_part = found
            scale = lax.rsqrt(jnp.sum(total, axis=1, keepdims=True) / full + EPSILON)
            gate_part = gate_part * scale
            share = 0.5 + 0.5 * jnp.tanh(0.5 * gate_part)
            hidden[role] = (gate_part * share * (up_part * scale)).astype(BF16)

    def descend(j, kind):
        level = flip(z, j)
        span = slice(groups - 1, groups) if kind else slice(0, groups - 1)
        count = 1 if kind else groups - 1
        left = hidden[span].reshape(count * cap, hidden.shape[2])

        def block(core):
            columns = pl.ds(pl.multiple_of((level * CORES + core) * width, 128), width)
            return jnp.dot(left, down[:, columns], preferred_element_type=F32)

        other, this = block(1 - c), block(c)
        half[level, span] = other.reshape(count, cap, width).astype(BF16)
        own[level, span] = this.reshape(count, cap, width)
        half_copy(level, kind).start()

    def finish(j, kind):
        level = flip(z, j)
        half_copy(level, kind).wait_recv()
        if j == 0:
            hand_copy(kind).wait_recv()
        for role in (groups - 1,) if kind else range(1, groups):
            role = role if kind else role % (groups - 1)
            found = own[level, role] + half_in[level, role].astype(F32)
            if j == 0:
                found = found + hand_in[role].astype(F32)
            if j == 1:
                hand[role] = found.astype(BF16)
            elif role:
                back[level, role - 1] = found.astype(BF16)
                back_copy(level, role).start()
            else:
                ret[level, 0] = found.astype(BF16)
        if j == 1:
            hand_copy(kind).start()

    def settle(j):
        level = flip(z, j)
        for role in range(groups - 1, 0, -1):
            back_copy(level, role).wait_recv()
        combined = jnp.dot(
            mix[...], ret[level].reshape(groups * cap, width), preferred_element_type=F32
        )
        found = []
        for h in range(HALVES):
            part = combined[h * (rows // HALVES) : (h + 1) * (rows // HALVES)]
            for source in {3: (), 2: (3,), 0: (2,)}[j]:
                sum_copy(source, h).wait_recv()
                arrived = zin[source, h * (rows // HALVES) : (h + 1) * (rows // HALVES)]
                part = part + arrived.astype(F32)
            if j:
                zsend[j, h * (rows // HALVES) : (h + 1) * (rows // HALVES)] = part.astype(BF16)
                sum_copy(j, h).start()
            found.append(part)
        return jnp.concatenate(found, axis=0)

    spread = plan_rows()
    pick(0)
    plan_mix(spread)
    spare = gains.at[pl.ds(0, parts - 1)]
    remote(spare, spare, gs, gr, tp=flip(t, 1)).wait_recv()
    inputs[4].wait()
    loads[0].wait()
    loads[1].wait()
    project(0)
    for h in range(PIECES):
        relay(1, h)
    pick(1)
    pass_on(0, 1)
    pass_on(0, 2)
    relay(2, 0)
    project(1)
    relay(2, 1)
    project(2)
    relay(2, 2)
    relay(2, 3)
    pick(2)
    pass_on(0, 3)
    relay(3, 0)
    relay(3, 1)
    project(3)
    relay(3, 2)
    relay(3, 3)
    pick(3)
    pass_on(1, 1)
    pass_on(1, 2)
    pass_on(1, 3)
    project(4)
    project(5)
    pass_on(2, 1)
    pass_on(2, 2)
    pass_on(2, 3)
    project(6)
    project(7)
    pass_on(3, 1)
    pass_on(3, 2)
    project(8)
    project(9)
    pass_on(3, 3)
    loads[2].wait()
    descend(3, 0)
    descend(1, 0)
    project(10)
    finish(3, 0)
    finish(1, 0)
    descend(3, 1)
    descend(1, 1)
    descend(2, 0)
    finish(3, 1)
    descend(2, 1)
    finish(2, 0)
    finish(2, 1)
    descend(0, 0)
    descend(0, 1)
    settle(3)
    finish(1, 1)
    finish(0, 0)
    settle(2)
    finish(0, 1)
    combined = settle(0)

    square = combined * combined
    folded = square[:, 0:128]
    for lane in range(128, width, 128):
        folded = folded + square[:, lane : lane + 128]
    stats[t] = jnp.sum(folded.T, axis=0, keepdims=True)
    for i in range(1, parts):
        stat_copy(i, t).start()
    def sent(ref, sem):
        remote(ref, ref, sem, sem, tp=flip(t, 1)).wait_send()

    for k in range(levels):

        @pl.when((z == k) & (z < levels - 1))
        def _():
            sent(zbuf.at[pl.ds(0, k + 1)], zs.at[1])

        @pl.when((z == k) & (z > 0))
        def _():
            sent(zbuf.at[pl.ds(0, levels - k)], zs.at[0])

    for ref, sem in (
        (xsend, ns), (x.at[pl.ds(0, levels)], fs), (half, ds), (hand, hs),
        (back.at[pl.ds(1, levels - 1)], qs), (zsend.at[pl.ds(2, levels - 2)], ts), (spare, gs),
    ):
        sent(ref, sem)
    seen = stats.at[pl.ds(0, parts - 1)]
    remote(seen, seen, ps, pr, tp=flip(t, 1)).wait_recv()
    total = jnp.sum(stats[...], axis=0)
    high = total.astype(BF16)
    ones = jnp.ones((1, 128), BF16)
    column = sum(
        lax.dot_general(v, ones, (((0,), (0,)), ((), ())), preferred_element_type=F32)
        for v in (high, (total - high.astype(F32)).astype(BF16))
    )
    scale = lax.rsqrt(column[:, 0:1] / full + EPSILON)
    out[...] = (combined * scale * post[...]).astype(BF16)
    sent(seen, ps)


def local_fused(tokens, pre_gain, expert_gate, expert_up, expert_down, routes, route_weights, post_gain):
    groups, parts = lax.axis_size("ep"), lax.axis_size("tp")
    rows, width = tokens.shape
    _, features, units = expert_gate.shape
    levels = parts // CORES
    cap = 3 * rows // groups
    vmem = pl.BlockSpec(memory_space=pltpu.VMEM)
    anywhere = pl.BlockSpec(memory_space=pl.ANY)
    dma = pltpu.SemaphoreType.DMA
    tok_block = pltpu.VMEM((levels, rows, width), BF16)
    block = (levels, groups, cap, width)
    away = pltpu.VMEM((levels, groups - 1, cap, width), BF16)
    return pl.pallas_call(
        functools.partial(fused, groups, parts),
        out_shape=pltpu.VMEM((rows, width), BF16),
        in_specs=[anywhere] * 8,
        out_specs=vmem,
        scratch_shapes=[
            tok_block,
            pltpu.VMEM((parts, 1, width), F32),
            pltpu.VMEM((2, rows), jnp.int32),
            pltpu.VMEM((2, rows), F32),
            pltpu.VMEM((1, width), F32),
            pltpu.VMEM((groups * cap, rows), BF16),
            pltpu.VMEM((rows, groups * cap), BF16),
            pltpu.VMEM((parts, groups, cap, width), BF16),
            away,
            pltpu.VMEM((groups, cap, 128), F32),
            pltpu.VMEM((features, units), BF16),
            pltpu.VMEM((features, units), BF16),
            pltpu.VMEM((units, features), BF16),
            pltpu.VMEM((groups, cap, units), F32),
            pltpu.VMEM((groups, cap, units), F32),
            pltpu.VMEM((groups, cap, units), BF16),
            pltpu.VMEM(block, BF16),
            pltpu.VMEM(block, BF16),
            pltpu.VMEM(block, F32),
            away,
            pltpu.VMEM(block, BF16),
            pltpu.VMEM((groups, cap, width), BF16),
            pltpu.VMEM((groups, cap, width), BF16),
            tok_block,
            tok_block,
            pltpu.VMEM((parts, 1, rows), F32),
            dma((5,)), dma((3,)),
            dma((2,)), dma((levels, PIECES)),
            dma, dma,
            dma, dma((levels, groups - 1)),
            dma, dma((len(BATCHES),)),
            dma, dma((levels, 2)),
            dma, dma((levels, groups - 1)),
            dma, dma((2,)),
            dma, dma((levels, HALVES)),
            dma, dma,
        ],
        compiler_params=pltpu.CompilerParams(
            collective_id=0, has_side_effects=True, vmem_limit_bytes=60 * 1024 * 1024
        ),
    )(
        tokens, pre_gain.reshape(1, width), routes.T, route_weights.T,
        expert_gate, expert_up, expert_down, post_gain.reshape(1, width),
    )


def plan(mesh):
    def choose(*args):
        tokens, gate = args[0], args[2]
        groups, parts = mesh.shape["ep"], mesh.shape["tp"]
        rows, width = tokens.shape
        fits = (
            gate.shape[0] == 1
            and groups == 4
            and parts == 4 * CORES
            and width % 128 == 0
            and rows % 128 == 0
            and (3 * rows // groups) % 64 == 0
            and gate.shape[2] % 128 == 0
        )
        return (local_fused if fits else local)(*args)

    return choose


def solution(mesh):
    placed = (
        P("ep", "tp"),
        P("tp"),
        P("ep", None, "tp"),
        P("ep", None, "tp"),
        P("ep", "tp", None),
        P("ep", None),
        P("ep", None),
        P("tp"),
    )
    return jax.shard_map(
        plan(mesh), mesh=mesh, in_specs=placed, out_specs=P("ep", "tp"), check_vma=False
    )
```

time: 67.1 us -> 55 us (0.82)
  Pallas kernels: 65.4 us -> 54.1 us
  local copies, waits for them, and re-layouts: 1.57 us -> 0.66 us
    pallas_call x1, Pallas kernels: 65.4 us -> 54.1 us  [local_fused(): pl.pallas_call(functools.partial(fused, groups, parts), out_shape=pltpu.V...]
    unnamed x1, local copies, waits for them, and re-layouts: 1.57 us -> 0.66 us
where the time goes in v2:
time: 55 us; the launch traced here: 54.8 us
  Pallas kernels  54.1 us (98%)
  local copies, waits for them, and re-layouts  0.66 us (1%)
    pallas_call x1, Pallas kernels, local_fused(): pl.pallas_call(functools.partial(fused, groups, parts), out_shape=pltpu.V...  54.1 us

profile of v2, /device:TPU:0, one launch (start us, length us, event | category | flops | bytes accessed | tf_op | source)
XLA Modules:
  0.0 54.8 jit_solution(4942470596713986868)
XLA Ops:
  0.0 54.1 %shard_map.82 = bf16[256,256]{1,0:T(8,128)(2,1)S(1)} custom-call(bf16[256,256]{1,0:T(8,128)(2,1)} %tok.1, f32[1,256]{1,0:T(1,128)} %bitcast.6, s32[2,256]{1,0:T(2,128)} %bitcast.4, f32[2,256]{1,0:T(2,128)} %bitcast.5, bf16[1,2048,1024]{2,1,0:T(8,128)(2,1)} %gate_hbm.1, bf16[1,2048,1024]{2,1,0:T(8,128)(2,1)} %up_hbm.1, bf16[1,1024,2048]{2,1,0:T(8,128)(2,1)} %down_hbm.1, ...), custom_call_target="tpu_custom_call" | custom-call | tf_op jit(solution)/shard_map/pallas_call | solution.py:458
  54.1 0.7 %copy.10 = bf16[256,256]{1,0:T(8,128)(2,1)} copy(bf16[256,256]{1,0:T(8,128)(2,1)S(1)} %shard_map.82) | data formatting | bytes 262144

commit v3 on v2

--- a/solution.py
+++ b/solution.py
@@ -64,7 +64,7 @@
 
 CORES = 2
 PIECES = 4
-HALVES = 2
+HALVES = 4
 F32 = jnp.float32
 BF16 = jnp.bfloat16
 MESH = pl.DeviceIdType.MESH
@@ -80,8 +80,8 @@
 
 
 BATCHES = (
-    ((0, 0),), ((0, 1),), ((1, 0), (2, 0)), ((3, 0), (0, 2)), ((1, 1), (2, 1)), ((3, 1), (0, 3)),
-    ((1, 2), (2, 2)), ((3, 2),), ((1, 3),), ((2, 3),), ((3, 3),),
+    ((0, 0), (0, 1)), ((1, 0), (2, 0)), ((3, 0), (0, 2)), ((1, 1), (2, 1)), ((0, 3),),
+    ((1, 2), (2, 2)), ((3, 1), (3, 2)), ((1, 3),), ((2, 3),), ((3, 3),),
 )
 
 
@@ -90,13 +90,13 @@
     zbuf, gains, route, weight, post, disp, mix, x, xsend, squares,
     gate, up, down, acc_gate, acc_up, hidden, half, half_in, own, back, ret,
     hand, hand_in, zsend, zin, stats,
-    isem, wsem, zs, zr, gs, gr, ns, nr, fs, fr, ds, dr, qs, qr, hs, hr, ts, tr, ps, pr,
+    isem, wsem, zs, zr, gs, gr, ns, nr, ks, kr, fs, fr, ds, dr, qs, qr, hs, hr, ts, tr, ps, pr,
 ):
     t, e = lax.axis_index("tp"), lax.axis_index("ep")
     z, c = lax.div(t, CORES), lax.rem(t, CORES)
     levels = parts // CORES
     rows, width = zbuf.shape[1:]
-    cap = xsend.shape[2]
+    cap = xsend.shape[1]
     full = parts * width
     around = [flip(e, role) if role else e for role in range(groups)]
     batch_of = {unit: k for k, batch in enumerate(BATCHES) for unit in batch}
@@ -162,7 +162,7 @@
 
     def row_copy(level, role, source):
         return remote(
-            xsend.at[level, role - 1], x.at[level * CORES + c, source],
+            xsend.at[level * (groups - 1) + role - 1], x.at[level * CORES + c, source],
             ns, nr.at[level, role - 1], ep=around[role],
         )
 
@@ -183,17 +183,17 @@
             qs, qr.at[level, role - 1], ep=around[role],
         )
 
-    def hand_copy(kind):
-        span = pl.ds(groups - 1, 1) if kind else pl.ds(0, groups - 1)
+    def hand_copy(k):
+        span = (pl.ds(1, groups - 2), pl.ds(groups - 1, 1), pl.ds(0, 1))[k]
         return remote(
-            hand.at[span], hand_in.at[span], hs, hr.at[kind], tp=flip(z, 1) * CORES + c
+            hand.at[span], hand_in.at[span], hs, hr.at[k], tp=flip(z, 1) * CORES + c
         )
 
     def sum_copy(j, h):
         bits = 2 if j == 2 else 1
         return remote(
             piece_of(zsend, j, h, HALVES), piece_of(zin, j, h, HALVES),
-            ts, tr.at[j, h], tp=flip(z, bits) * CORES + c,
+            ts, tr.at[j - 2, h], tp=flip(z, bits) * CORES + c,
         )
 
     def stat_copy(i, part):
@@ -238,14 +238,21 @@
         level = flip(z, j)
         picked = jnp.dot(disp[...], zbuf[level], preferred_element_type=F32).astype(BF16)
         for role in range(1, groups):
-            xsend[level, role - 1] = picked[role * cap : (role + 1) * cap]
+            xsend[level * (groups - 1) + role - 1] = picked[role * cap : (role + 1) * cap]
         x[level * CORES + c, e] = picked[:cap]
-        for role in range(1, groups):
+        for role in range(1, groups - 1 if j == 1 else groups):
             row_copy(level, role, e).start()
         core_copy(j, 0).start()
 
+    def along_copy(j):
+        slot = x.at[flip(z, j) * CORES + c, around[groups - 1]]
+        return remote(slot, slot, ks, kr, tp=flip(z, 1) * CORES + c)
+
     def pass_on(j, role):
-        row_copy(flip(z, j), role, around[role]).wait_recv()
+        if j == 1 and role == groups - 1:
+            along_copy(1).wait_recv()
+        else:
+            row_copy(flip(z, j), role, around[role]).wait_recv()
         core_copy(j, role).start()
 
     def level_sum(j, role):
@@ -302,27 +309,36 @@
     def finish(j, kind):
         level = flip(z, j)
         half_copy(level, kind).wait_recv()
+
+        def found(role):
+            rows_found = own[level, role] + half_in[level, role].astype(F32)
+            if j == 0:
+                rows_found = rows_found + hand_in[role].astype(F32)
+            return rows_found.astype(BF16)
+
         if j == 0:
             hand_copy(kind).wait_recv()
-        for role in (groups - 1,) if kind else range(1, groups):
-            role = role if kind else role % (groups - 1)
-            found = own[level, role] + half_in[level, role].astype(F32)
-            if j == 0:
-                found = found + hand_in[role].astype(F32)
+        for role in (groups - 1,) if kind else range(1, groups - 1):
             if j == 1:
-                hand[role] = found.astype(BF16)
-            elif role:
-                back[level, role - 1] = found.astype(BF16)
+                hand[role] = found(role)
+            else:
+                back[level, role - 1] = found(role)
                 back_copy(level, role).start()
-            else:
-                ret[level, 0] = found.astype(BF16)
-        if j == 1:
-            hand_copy(kind).start()
+        if j == 1 and kind == 0:
+            hand_copy(0).start()
+        if kind == 0 and j == 1:
+            hand[0] = found(0)
+        elif kind == 0 and j > 1:
+            ret[level, 0] = found(0)
+        elif kind == 0:
+            return found
+
+    def arrive(j, *roles):
+        for role in roles:
+            back_copy(flip(z, j), role).wait_recv()
 
     def settle(j):
         level = flip(z, j)
-        for role in range(groups - 1, 0, -1):
-            back_copy(level, role).wait_recv()
         combined = jnp.dot(
             mix[...], ret[level].reshape(groups * cap, width), preferred_element_type=F32
         )
@@ -342,66 +358,74 @@
     spread = plan_rows()
     pick(0)
     plan_mix(spread)
+    for h in range(PIECES):
+        relay(1, h)
+    pick(1)
     spare = gains.at[pl.ds(0, parts - 1)]
     remote(spare, spare, gs, gr, tp=flip(t, 1)).wait_recv()
     inputs[4].wait()
     loads[0].wait()
     loads[1].wait()
-    project(0)
-    for h in range(PIECES):
-        relay(1, h)
-    pick(1)
+    relay(2, 0)
     pass_on(0, 1)
     pass_on(0, 2)
-    relay(2, 0)
-    project(1)
     relay(2, 1)
-    project(2)
+    project(0)
     relay(2, 2)
     relay(2, 3)
     pick(2)
     pass_on(0, 3)
     relay(3, 0)
+    project(1)
     relay(3, 1)
-    project(3)
     relay(3, 2)
     relay(3, 3)
+    along_copy(0).start()
     pick(3)
     pass_on(1, 1)
     pass_on(1, 2)
+    project(2)
+    project(3)
+    project(4)
     pass_on(1, 3)
-    project(4)
-    project(5)
     pass_on(2, 1)
     pass_on(2, 2)
     pass_on(2, 3)
+    project(5)
+    pass_on(3, 1)
     project(6)
+    pass_on(3, 2)
     project(7)
-    pass_on(3, 1)
-    pass_on(3, 2)
     project(8)
-    project(9)
     pass_on(3, 3)
     loads[2].wait()
     descend(3, 0)
+    project(9)
+    descend(3, 1)
+    finish(3, 0)
     descend(1, 0)
-    project(10)
-    finish(3, 0)
-    finish(1, 0)
-    descend(3, 1)
+    finish(3, 1)
     descend(1, 1)
     descend(2, 0)
-    finish(3, 1)
+    finish(1, 0)
     descend(2, 1)
+    finish(1, 1)
+    hand_copy(1).start()
+    descend(0, 0)
+    descend(0, 1)
+    arrive(3, 1, 2)
     finish(2, 0)
     finish(2, 1)
-    descend(0, 0)
-    descend(0, 1)
+    arrive(3, 3)
     settle(3)
-    finish(1, 1)
-    finish(0, 0)
+    rest = finish(0, 0)
+    arrive(2, 1, 2, 3)
+    finish(0, 1)
     settle(2)
-    finish(0, 1)
+    hand_copy(2).start()
+    hand_copy(2).wait_recv()
+    ret[z, 0] = rest(0)
+    arrive(0, 1, 2, 3)
     combined = settle(0)
 
     square = combined * combined
@@ -425,7 +449,8 @@
             sent(zbuf.at[pl.ds(0, levels - k)], zs.at[0])
 
     for ref, sem in (
-        (xsend, ns), (x.at[pl.ds(0, levels)], fs), (half, ds), (hand, hs),
+        (xsend.at[pl.ds(0, levels * (groups - 1) - 1)], ns), (x.at[0, 0], ks),
+        (x.at[pl.ds(0, levels)], fs), (half, ds), (hand, hs),
         (back.at[pl.ds(1, levels - 1)], qs), (zsend.at[pl.ds(2, levels - 2)], ts), (spare, gs),
     ):
         sent(ref, sem)
@@ -469,7 +494,7 @@
             pltpu.VMEM((groups * cap, rows), BF16),
             pltpu.VMEM((rows, groups * cap), BF16),
             pltpu.VMEM((parts, groups, cap, width), BF16),
-            away,
+            pltpu.VMEM((levels * (groups - 1), cap, width), BF16),
             pltpu.VMEM((groups, cap, 128), F32),
             pltpu.VMEM((features, units), BF16),
             pltpu.VMEM((features, units), BF16),
@@ -491,11 +516,12 @@
             dma((2,)), dma((levels, PIECES)),
             dma, dma,
             dma, dma((levels, groups - 1)),
+            dma, dma,
             dma, dma((len(BATCHES),)),
             dma, dma((levels, 2)),
             dma, dma((levels, groups - 1)),
-            dma, dma((2,)),
-            dma, dma((levels, HALVES)),
+            dma, dma((3,)),
+            dma, dma((2, HALVES)),
             dma, dma,
         ],
         compiler_params=pltpu.CompilerParams(

time: 55 us -> 53.7 us (0.976)
  Pallas kernels: 54.1 us -> 52.8 us
    pallas_call x1, Pallas kernels: 54.1 us -> 52.8 us  [local_fused(): pl.pallas_call(functools.partial(fused, groups, parts), out_shape=pltpu.V...]
where the time goes in v3:
time: 53.7 us; the launch traced here: 53.5 us
  Pallas kernels  52.8 us (98%)
  local copies, waits for them, and re-layouts  0.66 us (1%)
    pallas_call x1, Pallas kernels, local_fused(): pl.pallas_call(functools.partial(fused, groups, parts), out_shape=pltpu.V...  52.8 us

profile of v3, /device:TPU:0, one launch (start us, length us, event | category | flops | bytes accessed | tf_op | source)
XLA Modules:
  0.0 53.5 jit_solution(1808847066135782924)
XLA Ops:
  0.0 52.8 %shard_map.82 = bf16[256,256]{1,0:T(8,128)(2,1)S(1)} custom-call(bf16[256,256]{1,0:T(8,128)(2,1)} %tok.1, f32[1,256]{1,0:T(1,128)} %bitcast.6, s32[2,256]{1,0:T(2,128)} %bitcast.4, f32[2,256]{1,0:T(2,128)} %bitcast.5, bf16[1,2048,1024]{2,1,0:T(8,128)(2,1)} %gate_hbm.1, bf16[1,2048,1024]{2,1,0:T(8,128)(2,1)} %up_hbm.1, bf16[1,1024,2048]{2,1,0:T(8,128)(2,1)} %down_hbm.1, ...), custom_call_target="tpu_custom_call" | custom-call | tf_op jit(solution)/shard_map/pallas_call | solution.py:483
  52.8 0.7 %copy.10 = bf16[256,256]{1,0:T(8,128)(2,1)} copy(bf16[256,256]{1,0:T(8,128)(2,1)S(1)} %shard_map.82) | data formatting | bytes 262144

commit v4 on v3

--- a/solution.py
+++ b/solution.py
@@ -370,10 +370,10 @@
     pass_on(0, 1)
     pass_on(0, 2)
     relay(2, 1)
-    project(0)
     relay(2, 2)
     relay(2, 3)
     pick(2)
+    project(0)
     pass_on(0, 3)
     relay(3, 0)
     project(1)
@@ -400,27 +400,26 @@
     pass_on(3, 3)
     loads[2].wait()
     descend(3, 0)
+    descend(1, 0)
     project(9)
+    finish(3, 0)
     descend(3, 1)
-    finish(3, 0)
-    descend(1, 0)
+    descend(1, 1)
+    finish(1, 0)
+    descend(2, 0)
     finish(3, 1)
-    descend(1, 1)
-    descend(2, 0)
-    finish(1, 0)
     descend(2, 1)
     finish(1, 1)
     hand_copy(1).start()
     descend(0, 0)
     descend(0, 1)
-    arrive(3, 1, 2)
     finish(2, 0)
     finish(2, 1)
-    arrive(3, 3)
+    arrive(3, 1, 2, 3)
     settle(3)
     rest = finish(0, 0)
+    finish(0, 1)
     arrive(2, 1, 2, 3)
-    finish(0, 1)
     settle(2)
     hand_copy(2).start()
     hand_copy(2).wait_recv()

time: 53.7 us -> 53.1 us (0.989)
  no operation moved by 1% of the time
where the time goes in v4:
time: 53.1 us; the launch traced here: 53 us
  Pallas kernels  52.3 us (98%)
  local copies, waits for them, and re-layouts  0.66 us (1%)
    pallas_call x1, Pallas kernels, local_fused(): pl.pallas_call(functools.partial(fused, groups, parts), out_shape=pltpu.V...  52.3 us

profile of v4, /device:TPU:0, one launch (start us, length us, event | category | flops | bytes accessed | tf_op | source)
XLA Modules:
  0.0 53.0 jit_solution(4333480970043531002)
XLA Ops:
  0.0 52.3 %shard_map.82 = bf16[256,256]{1,0:T(8,128)(2,1)S(1)} custom-call(bf16[256,256]{1,0:T(8,128)(2,1)} %tok.1, f32[1,256]{1,0:T(1,128)} %bitcast.6, s32[2,256]{1,0:T(2,128)} %bitcast.4, f32[2,256]{1,0:T(2,128)} %bitcast.5, bf16[1,2048,1024]{2,1,0:T(8,128)(2,1)} %gate_hbm.1, bf16[1,2048,1024]{2,1,0:T(8,128)(2,1)} %up_hbm.1, bf16[1,1024,2048]{2,1,0:T(8,128)(2,1)} %down_hbm.1, ...), custom_call_target="tpu_custom_call" | custom-call | tf_op jit(solution)/shard_map/pallas_call | solution.py:482
  52.3 0.7 %copy.10 = bf16[256,256]{1,0:T(8,128)(2,1)} copy(bf16[256,256]{1,0:T(8,128)(2,1)S(1)} %shard_map.82) | data formatting | bytes 262144

commit v5 on v4

--- a/solution.py
+++ b/solution.py
@@ -64,7 +64,7 @@
 
 CORES = 2
 PIECES = 4
-HALVES = 4
+HALVES = 2
 F32 = jnp.float32
 BF16 = jnp.bfloat16
 MESH = pl.DeviceIdType.MESH
@@ -180,7 +180,7 @@
     def back_copy(level, role):
         return remote(
             back.at[level, role - 1], ret.at[level, role],
-            qs, qr.at[level, role - 1], ep=around[role],
+            qs, qr.at[level], ep=around[role],
         )
 
     def hand_copy(k):
@@ -333,9 +333,10 @@
         elif kind == 0:
             return found
 
-    def arrive(j, *roles):
-        for role in roles:
-            back_copy(flip(z, j), role).wait_recv()
+    def arrive(j):
+        level = flip(z, j)
+        found = ret.at[level, pl.ds(1, groups - 1)]
+        remote(found, found, qs, qr.at[level], ep=around[1]).wait_recv()
 
     def settle(j):
         level = flip(z, j)
@@ -415,16 +416,16 @@
     descend(0, 1)
     finish(2, 0)
     finish(2, 1)
-    arrive(3, 1, 2, 3)
+    arrive(3)
     settle(3)
     rest = finish(0, 0)
     finish(0, 1)
-    arrive(2, 1, 2, 3)
+    arrive(2)
     settle(2)
     hand_copy(2).start()
     hand_copy(2).wait_recv()
     ret[z, 0] = rest(0)
-    arrive(0, 1, 2, 3)
+    arrive(0)
     combined = settle(0)
 
     square = combined * combined
@@ -518,7 +519,7 @@
             dma, dma,
             dma, dma((len(BATCHES),)),
             dma, dma((levels, 2)),
-            dma, dma((levels, groups - 1)),
+            dma, dma((levels,)),
             dma, dma((3,)),
             dma, dma((2, HALVES)),
             dma, dma,

time: 53.1 us -> 53 us (level)
  no operation moved by 1% of the time
where the time goes in v5:
time: 53 us; the launch traced here: 52.9 us
  Pallas kernels  52.2 us (98%)
  local copies, waits for them, and re-layouts  0.66 us (1%)
    pallas_call x1, Pallas kernels, local_fused(): pl.pallas_call(functools.partial(fused, groups, parts), out_shape=pltpu.V...  52.2 us

profile of v5, /device:TPU:0, one launch (start us, length us, event | category | flops | bytes accessed | tf_op | source)
XLA Modules:
  0.0 52.9 jit_solution(4594809916389195699)
XLA Ops:
  0.0 52.2 %shard_map.82 = bf16[256,256]{1,0:T(8,128)(2,1)S(1)} custom-call(bf16[256,256]{1,0:T(8,128)(2,1)} %tok.1, f32[1,256]{1,0:T(1,128)} %bitcast.6, s32[2,256]{1,0:T(2,128)} %bitcast.4, f32[2,256]{1,0:T(2,128)} %bitcast.5, bf16[1,2048,1024]{2,1,0:T(8,128)(2,1)} %gate_hbm.1, bf16[1,2048,1024]{2,1,0:T(8,128)(2,1)} %up_hbm.1, bf16[1,1024,2048]{2,1,0:T(8,128)(2,1)} %down_hbm.1, ...), custom_call_target="tpu_custom_call" | custom-call | tf_op jit(solution)/shard_map/pallas_call | solution.py:483
  52.2 0.7 %copy.10 = bf16[256,256]{1,0:T(8,128)(2,1)} copy(bf16[256,256]{1,0:T(8,128)(2,1)S(1)} %shard_map.82) | data formatting | bytes 262144
